TPU v7x, 512 devices: a whole 4x8x8 slice. The times are simulated.
512 devices in a mesh: ep: 32 (over z, x), tp: 16 (over y, core).
Axes of the slice: x: 4, y: 8, z: 8, core: 2. Of those that a mesh axis runs over, the one named last changes fastest.
Arguments:
- tokens: bfloat16 [1024, 2048], P(('ep', 'tp')), may hold values from -6 to 6
- cache_keys: bfloat16 [1024, 1024, 256], P(('ep', 'tp')), may hold values from -360 to 360
- cache_values: bfloat16 [1024, 1024, 256], P(('ep', 'tp')), may hold values from -6 to 6
- cache_gates: float32 [1024, 2, 1024], P(('ep', 'tp')), may hold values from -256 to 0, as said below
- lengths: int32 [1024], P(('ep', 'tp')), may hold values from 1 to 1024, 524288 in all
- routes: int32 [1024, 4], P(('ep', 'tp')), may hold values from 0 to 31, all different within a row; in each aligned block of 2 rows (0 to 1, 2 to 3, ...) no two rows name the same one
- route_logits: float32 [1024, 4], P(('ep', 'tp')), may hold values from -6 to 6
- attn_gain: float32 [2048], replicated, may hold values from 0.1 to 1.9
- w_query: bfloat16 [2048, 2048], P(None, 'tp'), may hold values from -0.125 to 0.125
- w_keyval: bfloat16 [2048, 512], P(None, 'tp'), may hold values from -0.125 to 0.125
- w_forget: bfloat16 [2048, 2], replicated, may hold values from -0.125 to 0.125
- forget_bias: float32 [2], replicated, may hold values from -1 to 3
- w_out: bfloat16 [2048, 2048], P(None, 'tp'), may hold values from -0.125 to 0.125
- mix_gain: float32 [2048], replicated, may hold values from 0.1 to 1.9
- ffn_gain: float32 [2048], replicated, may hold values from 0.1 to 1.9
- w_gate: bfloat16 [32, 2048, 2048], P('ep', None, 'tp'), may hold values from -0.125 to 0.125
- w_lin: bfloat16 [32, 2048, 2048], P('ep', None, 'tp'), may hold values from -0.125 to 0.125
- gate_bias: float32 [32, 2048], P('ep', 'tp'), may hold values from -12 to 12
- lin_bias: float32 [32, 2048], P('ep', 'tp'), may hold values from -12 to 12
- w_down: bfloat16 [32, 2048, 2048], P('ep', 'tp'), may hold values from -0.125 to 0.125
- post_gain: float32 [2048], replicated, may hold values from 0.1 to 1.9
Outputs:
- updated: bfloat16 [1024, 2048], P(('ep', 'tp'))
- new_entries: bfloat16 [1024, 512], P(('ep', 'tp'))
Inputs may be any that keep to these rules, and one draw needn't show every extreme that they name: `cache_gates`: along the positions of each sequence and head the values never increase. The lengths of all sequences add up to 524288, and some sequence has exactly 1024. `routes`: each row names 4 different experts; among the rows of one device no expert is named twice; every expert is named by some row.
All inputs are finite; a program needn't handle non-finite values. No bound on the sum of `lengths` on one device may be relied on, other than what follows from the above.
Results may differ from a plain program's by a relative error of at most 0.014.
The roundings to bfloat16 on the way count: a program that leaves them out, or rounds other values in their place, can miss the bound.
Values may be sent and summed in bfloat16 or wider, within the bound.
A program may use at most 64 MiB of HBM per device.

v0:
```python
import jax
import jax.numpy as jnp
from jax import lax
from jax.sharding import PartitionSpec as P

HEADS = 16
KVH = 2
HDIM = 128
NORM_EPS = 1e-06
SWIGLU_ALPHA = 1.702
SWIGLU_LIMIT = 7.0
NEG_LARGE = -1e30


def laid_out(tiles, dim):
    shape = list(tiles.shape[1:])
    shape[dim] *= tiles.shape[0]
    return jnp.moveaxis(tiles, 0, dim).reshape(shape)


def sent_to_all(array, axis):
    copies = jnp.broadcast_to(array, (lax.axis_size(axis), *array.shape))
    return lax.all_to_all(copies, axis, split_axis=0, concat_axis=0, tiled=True)


def gather_directly(array, axis, dim):
    return laid_out(sent_to_all(array, axis), dim)


def rms_scale(values, gain):
    values = values.astype(jnp.float32)
    return values * lax.rsqrt(jnp.mean(values * values, axis=-1, keepdims=True) + NORM_EPS) * gain


def clamped_unit(gate, linear):
    gate = jnp.minimum(gate, SWIGLU_LIMIT)
    linear = jnp.clip(linear, -SWIGLU_LIMIT, SWIGLU_LIMIT)
    return gate * jax.nn.sigmoid(SWIGLU_ALPHA * gate) * (linear + 1.0)


def block_scores(q_four, cache_keys, cache_gates, base, lengths, span, scale):
    seqs = cache_keys.shape[0]
    k_four = cache_keys.reshape(seqs, span, q_four.shape[1], q_four.shape[3])
    scores = (
        jnp.einsum("sgqd,spgd->sgqp", q_four, k_four, preferred_element_type=jnp.float32) * scale
    )
    scores = scores + (base[:, :, None, None] - cache_gates[:, :, None, :])
    place = lax.iota(jnp.int32, span)
    live = place[None, None, None, :] < lengths[:, None, None, None]
    return (jnp.where(live, scores, NEG_LARGE), live)


def per_device(
    tokens,
    cache_keys,
    cache_values,
    cache_gates,
    lengths,
    routes,
    route_logits,
    attn_gain,
    w_query,
    w_keyval,
    w_forget,
    forget_bias,
    w_out,
    mix_gain,
    ffn_gain,
    w_gate,
    w_lin,
    gate_bias,
    lin_bias,
    w_down,
    post_gain,
):
    seqs, width = tokens.shape
    normed = rms_scale(tokens, attn_gain).astype(jnp.bfloat16)
    query_cols = w_query.shape[1]
    pair_cols = w_keyval.shape[1]
    piece = gather_directly(normed, "tp", 0)
    both = jnp.concatenate(
        [
            jnp.dot(piece, w_query, preferred_element_type=jnp.float32),
            jnp.dot(piece, w_keyval, preferred_element_type=jnp.float32),
        ],
        axis=1,
    )
    gathered = both.astype(jnp.bfloat16)
    owned = lax.all_to_all(gathered, "tp", split_axis=0, concat_axis=1, tiled=True)
    groups = lax.axis_size("tp")
    owned = owned.reshape(seqs, groups, query_cols + pair_cols)
    query = owned[:, :, :query_cols].reshape(seqs, groups * query_cols)
    fresh = owned[:, :, query_cols:].reshape(seqs, groups * pair_cols)
    forget = jax.nn.log_sigmoid(
        jnp.dot(normed, w_forget, preferred_element_type=jnp.float32) + forget_bias
    )
    q_four = query.reshape(seqs, KVH, HEADS // KVH, HDIM)
    new_key = fresh[:, : KVH * HDIM].reshape(seqs, KVH, HDIM)
    new_value = fresh[:, KVH * HDIM :].reshape(seqs, KVH, HDIM)
    span_all = cache_keys.shape[1]
    place = lax.iota(jnp.int32, span_all)
    last = jnp.sum(
        jnp.where(place[None, None, :] == lengths[:, None, None] - 1, cache_gates, 0.0), axis=2
    )
    base = last + forget
    scale = HDIM ** (-0.5)
    own = jnp.einsum("sgqd,sgd->sgq", q_four, new_key, preferred_element_type=jnp.float32) * scale
    values_four = cache_values.reshape(seqs, span_all, KVH, HDIM)
    masked, live = block_scores(q_four, cache_keys, cache_gates, base, lengths, span_all, scale)
    top = jnp.maximum(jnp.max(masked, axis=-1), own)
    expo = jnp.where(live, jnp.exp(masked - top[..., None]), 0.0)
    own_expo = jnp.exp(own - top)
    total = jnp.sum(expo, axis=-1) + own_expo
    weights = (expo / total[..., None]).astype(jnp.bfloat16)
    mixed = jnp.einsum("sgqp,spgd->sgqd", weights, values_four, preferred_element_type=jnp.float32)
    own_weight = (own_expo / total).astype(jnp.bfloat16)
    mixed = (
        mixed
        + own_weight.astype(jnp.float32)[..., None] * new_value.astype(jnp.float32)[:, :, None, :]
    )
    mixed = mixed.reshape(seqs, HEADS * HDIM).astype(jnp.bfloat16)
    projected = jnp.dot(
        gather_directly(mixed, "tp", 0), w_out, preferred_element_type=jnp.float32
    ).astype(jnp.bfloat16)
    projected = lax.all_to_all(projected, "tp", split_axis=0, concat_axis=1, tiled=True)
    residual = tokens.astype(jnp.float32) + rms_scale(projected, mix_gain)
    expert_in = rms_scale(residual, ffn_gain).astype(jnp.bfloat16)
    experts = lax.axis_size("ep")
    hit = (routes[:, :, None] == lax.iota(jnp.int32, experts)[None, None, :]).astype(jnp.float32)
    probs = jax.nn.softmax(route_logits, axis=-1)
    combine = jnp.sum(probs[:, :, None] * hit, axis=1)
    chosen = jnp.sum(hit, axis=1).T
    outbound = jnp.dot(
        chosen.astype(jnp.bfloat16), expert_in, preferred_element_type=jnp.float32
    ).astype(jnp.bfloat16)[:, None, :]
    slots = outbound.shape[1]
    arrived = lax.all_to_all(outbound, "ep", split_axis=0, concat_axis=0, tiled=True)
    flat = arrived.reshape(experts * slots, width)
    pooled = lax.all_gather(flat, "tp", axis=0, tiled=True)
    piece = pooled
    gate = jnp.dot(piece, w_gate[0], preferred_element_type=jnp.float32) + gate_bias[0]
    linear = jnp.dot(piece, w_lin[0], preferred_element_type=jnp.float32) + lin_bias[0]
    act = clamped_unit(gate, linear).astype(jnp.bfloat16)
    summed = lax.psum_scatter(
        jnp.dot(act, w_down[0], preferred_element_type=jnp.float32).astype(jnp.bfloat16),
        "tp",
        scatter_dimension=0,
        tiled=True,
    )
    returned = lax.all_to_all(
        summed.reshape(experts, slots, width), "ep", split_axis=0, concat_axis=0, tiled=True
    )
    moe = jnp.einsum("se,ed->sd", combine, returned[:, 0, :].astype(jnp.float32))
    updated = (residual + rms_scale(moe, post_gain)).astype(jnp.bfloat16)
    return (updated, fresh)


def solution(mesh):
    in_specs = (
        P(("ep", "tp"), None),
        P(("ep", "tp"), None, None),
        P(("ep", "tp"), None, None),
        P(("ep", "tp"), None, None),
        P(("ep", "tp")),
        P(("ep", "tp"), None),
        P(("ep", "tp"), None),
        P(),
        P(None, "tp"),
        P(None, "tp"),
        P(),
        P(),
        P(None, "tp"),
        P(),
        P(),
        P("ep", None, "tp"),
        P("ep", None, "tp"),
        P("ep", "tp"),
        P("ep", "tp"),
        P("ep", "tp", None),
        P(),
    )
    out_specs = (P(("ep", "tp"), None), P(("ep", "tp"), None))
    return jax.shard_map(
        per_device, mesh=mesh, in_specs=in_specs, out_specs=out_specs, check_vma=False
    )
```

profile of v0, /device:TPU:25, one launch (start us, length us, event | category | flops | bytes accessed | tf_op | source)
XLA Modules:
  0.0 220.4 jit_solution(12834729480745042205)
XLA Ops:
  7.2 1.0 fusion.67
  8.2 0.8 fusion.69
  9.7 9.2 %all-to-all-start = ((bf16[16,2,2048]{2,1,0:T(2,128)(2,1)}), bf16[16,2,2048]{2,1,0:T(2,128)(2,1)S(1)}, u32[]{:S(2)}, u32[]{:S(2)}) async-start(bf16[16,2,2048]{2,1,0:T(2,128)(2,1)} %broadcast_in_dim.37), calls=%async_computation | async-start | bytes 262144 | tf_op jit(solution)/shard_map/all_to_all | solution.py:23
  19.6 0.8 select_reduce_fusion
  20.4 0.8 fusion.77
  21.3 0.8 broadcast_subtract_fusion
  22.1 3.2 %all-to-all-done = bf16[16,2,2048]{2,1,0:T(2,128)(2,1)S(1)} async-done(((bf16[16,2,2048]{2,1,0:T(2,128)(2,1)}), bf16[16,2,2048]{2,1,0:T(2,128)(2,1)S(1)}, u32[]{:S(2)}, u32[]{:S(2)}) %all-to-all-start) | async-done | bytes 131104 | tf_op jit(solution)/shard_map/all_to_all | solution.py:23
  25.2 1.1 convolution_convert_fusion.3
  26.3 1.3 convolution_convert_fusion.4
  28.2 5.8 %all-to-all-start.1 = ((bf16[16,2,160]{2,1,0:T(2,128)(2,1)}), bf16[16,2,160]{2,1,0:T(2,128)(2,1)S(1)}, u32[]{:S(2)}, u32[]{:S(2)}) async-start(bf16[16,2,160]{2,1,0:T(2,128)(2,1)} %copy.45), calls=%async_computation.1 | async-start | bytes 32768 | tf_op jit(solution)/shard_map/all_to_all | solution.py:89
  34.7 0.8 reduce_max.19
  35.5 3.0 %all-to-all-done.1 = bf16[16,2,160]{2,1,0:T(2,128)(2,1)S(1)} async-done(((bf16[16,2,160]{2,1,0:T(2,128)(2,1)}), bf16[16,2,160]{2,1,0:T(2,128)(2,1)S(1)}, u32[]{:S(2)}, u32[]{:S(2)}) %all-to-all-start.1) | async-done | bytes 10272 | tf_op jit(solution)/shard_map/all_to_all | solution.py:89
  40.6 6.6 %all-to-all-start.2 = ((bf16[16,2,2048]{2,1,0:T(2,128)(2,1)}), bf16[16,2,2048]{2,1,0:T(2,128)(2,1)S(1)}, u32[]{:S(2)}, u32[]{:S(2)}) async-start(bf16[16,2,2048]{2,1,0:T(2,128)(2,1)} %broadcast_in_dim.42), calls=%async_computation.2 | async-start | bytes 262144 | tf_op jit(solution)/shard_map/all_to_all | solution.py:23
  47.4 6.1 %all-to-all-done.2 = bf16[16,2,2048]{2,1,0:T(2,128)(2,1)S(1)} async-done(((bf16[16,2,2048]{2,1,0:T(2,128)(2,1)}), bf16[16,2,2048]{2,1,0:T(2,128)(2,1)S(1)}, u32[]{:S(2)}, u32[]{:S(2)}) %all-to-all-start.2) | async-done | bytes 131104 | tf_op jit(solution)/shard_map/all_to_all | solution.py:23
  53.6 0.8 convolution_convert_fusion.2
  54.4 5.7 %all-to-all-start.3 = ((bf16[16,2,128]{2,1,0:T(2,128)(2,1)}), bf16[16,2,128]{2,1,0:T(2,128)(2,1)S(1)}, u32[]{:S(2)}, u32[]{:S(2)}) async-start(bf16[16,2,128]{2,1,0:T(2,128)(2,1)} %bitcast.6), calls=%async_computation.3 | async-start | bytes 16384 | tf_op jit(solution)/shard_map/all_to_all | solution.py:125
  60.2 4.0 %all-to-all-done.3 = bf16[16,2,128]{2,1,0:T(2,128)(2,1)S(1)} async-done(((bf16[16,2,128]{2,1,0:T(2,128)(2,1)}), bf16[16,2,128]{2,1,0:T(2,128)(2,1)S(1)}, u32[]{:S(2)}, u32[]{:S(2)}) %all-to-all-start.3) | async-done | bytes 8224 | tf_op jit(solution)/shard_map/all_to_all | solution.py:125
  66.1 20.5 %all_to_all.46 = bf16[32,2,1024]{2,1,0:T(2,128)(2,1)S(1)} all-to-all(bf16[32,2,1024]{2,1,0:T(2,128)(2,1)S(1)} %reshape.160), channel_id=1, replica_groups=mesh['ep'=32,'tp'=16] {'ep'}, dimensions={0} | all-to-all | bytes 262144 | tf_op jit(solution)/shard_map/all_to_all | solution.py:137
  87.5 36.1 %all-gather.3.cloned.1.call-done = bf16[512,1,2048]{2,0,1:T(8,128)(2,1)} async-done(((bf16[32,1,2048]{2,0,1:T(8,128)(2,1)}), bf16[512,1,2048]{2,0,1:T(8,128)(2,1)}) %all-gather.3.cloned.1.call-update) | async-done | bytes 2097168 | tf_op jit(solution)/shard_map/all_gather | solution.py:139
  123.7 2.5 %fusion.8 = f32[512,128]{1,0:T(8,128)S(1)} fusion(bf16[512,1,2048]{2,0,1:T(8,128)(2,1)} %all-gather.3.cloned.1.call-done, bf16[1,2048,128]{2,1,0:T(8,128)(2,1)} %param.36, f32[128]{0:T(128)S(1)} %bitcast.104), kind=kOutput, calls=%fused_computation.8 | convolution fusion | flops 268566528 | bytes 2884096 | tf_op jit(solution)/shard_map/dot_general | solution.py:141
  126.2 3.8 %convolution_convert_fusion = bf16[512,2048]{1,0:T(8,128)(2,1)} fusion(bf16[512,1,2048]{2,0,1:T(8,128)(2,1)S(1)} %copy-done.1, bf16[1,128,2048]{2,1,0:T(8,128)(2,1)} %param.40, bf16[1,2048,128]{2,1,0:T(8,128)(2,1)} %param.37, f32[512,128]{1,0:T(8,128)S(1)} %fusion.8, f32[128]{0:T(128)S(1)} %bitcast.105), kind=kOutput, calls=%fused_computation | convolution fusion | flops 538574848 | bytes 5505536 | tf_op jit(solution)/shard_map/dot_general | solution.py:145
  130.1 61.4 %reduce-scatter.2.cloned.1.call-done = bf16[32,2048]{1,0:T(8,128)(2,1)} async-done(((bf16[512,2048]{1,0:T(8,128)(2,1)}), bf16[32,2048]{1,0:T(8,128)(2,1)}) %reduce-scatter.2.cloned.1.call-update) | async-done | bytes 131088 | tf_op jit(solution)/shard_map/reduce_scatter | solution.py:144
  191.5 1.6 reduce.3
  193.1 19.3 %all_to_all.47 = bf16[32,2,1024]{2,1,0:T(2,128)(2,1)S(1)} all-to-all(bf16[32,2,1024]{2,1,0:T(2,128)(2,1)S(1)} %reshape.162), channel_id=1, replica_groups=mesh['ep'=32,'tp'=16] {'ep'}, dimensions={0} | all-to-all | bytes 262144 | tf_op jit(solution)/shard_map/all_to_all | solution.py:150
  (71 shorter events, 9.2 us)
Async XLA Ops:
  7.2 31.6 %copy-start = (bf16[2,1024,256]{2,1,0:T(8,128)(2,1)S(1)}, bf16[2,1024,256]{2,1,0:T(8,128)(2,1)}, u32[]{:S(2)}) copy-start(bf16[2,1024,256]{2,1,0:T(8,128)(2,1)} %param.22) | copy-start | bytes 3145732
  7.2 32.3 %copy-start.12 = (bf16[2,1024,256]{2,1,0:T(8,128)(2,1)S(1)}, bf16[2,1024,256]{2,1,0:T(8,128)(2,1)}, u32[]{:S(2)}) copy-start(bf16[2,1024,256]{2,1,0:T(8,128)(2,1)} %param.23) | copy-start | bytes 3145732
  9.7 15.6 %all-to-all-start = ((bf16[16,2,2048]{2,1,0:T(2,128)(2,1)}), bf16[16,2,2048]{2,1,0:T(2,128)(2,1)S(1)}, u32[]{:S(2)}, u32[]{:S(2)}) async-start(bf16[16,2,2048]{2,1,0:T(2,128)(2,1)} %broadcast_in_dim.37), calls=%async_computation | async-start | bytes 262144 | tf_op jit(solution)/shard_map/all_to_all | solution.py:23
  26.3 20.8 %copy-start.4 = (f32[2,4]{1,0:T(2,128)S(1)}, f32[2,4]{1,0:T(2,128)}, u32[]{:S(2)}) copy-start(f32[2,4]{1,0:T(2,128)} %param.27) | copy-start | bytes 100
  27.6 25.9 %copy-start.2 = (bf16[2048,128]{1,0:T(8,128)(2,1)S(1)}, bf16[2048,128]{1,0:T(8,128)(2,1)}, u32[]{:S(2)}) copy-start(bf16[2048,128]{1,0:T(8,128)(2,1)} %param.33) | copy-start | bytes 1572868
  28.2 10.3 %all-to-all-start.1 = ((bf16[16,2,160]{2,1,0:T(2,128)(2,1)}), bf16[16,2,160]{2,1,0:T(2,128)(2,1)S(1)}, u32[]{:S(2)}, u32[]{:S(2)}) async-start(bf16[16,2,160]{2,1,0:T(2,128)(2,1)} %copy.45), calls=%async_computation.1 | async-start | bytes 32768 | tf_op jit(solution)/shard_map/all_to_all | solution.py:89
  38.6 15.7 %copy-start.7 = (bf16[2,512]{1,0:T(2,128)(2,1)}, bf16[2,512]{1,0:T(2,128)(2,1)S(1)}, u32[]{:S(2)}) copy-start(bf16[2,512]{1,0:T(2,128)(2,1)S(1)} %reshape.145) | copy-start | bytes 6148
  38.8 21.3 %copy-start.9 = (s32[2,4]{1,0:T(2,128)S(1)}, s32[2,4]{1,0:T(2,128)}, u32[]{:S(2)}) copy-start(s32[2,4]{1,0:T(2,128)} %param.26) | copy-start | bytes 100
  38.8 25.6 %copy-start.3 = (bf16[2,2048]{1,0:T(2,128)(2,1)S(1)}, bf16[2,2048]{1,0:T(2,128)(2,1)}, u32[]{:S(2)}) copy-start(bf16[2,2048]{1,0:T(2,128)(2,1)} %param.21) | copy-start | bytes 24580
  38.8 25.6 %copy-start.8 = (f32[2048]{0:T(1024)S(1)}, f32[2048]{0:T(1024)}, u32[]{:S(2)}) copy-start(f32[2048]{0:T(1024)} %param.34) | copy-start | bytes 24580
  38.8 25.8 %copy-start.5 = (f32[2048]{0:T(1024)S(1)}, f32[2048]{0:T(1024)}, u32[]{:S(2)}) copy-start(f32[2048]{0:T(1024)} %param.35) | copy-start | bytes 24580
  39.5 84.2 %copy-start.10 = (f32[1,128]{1,0:T(1,128)S(1)}, f32[1,128]{1,0:T(1,128)}, u32[]{:S(2)}) copy-start(f32[1,128]{1,0:T(1,128)} %param.38) | copy-start | bytes 1540
  40.6 12.9 %all-to-all-start.2 = ((bf16[16,2,2048]{2,1,0:T(2,128)(2,1)}), bf16[16,2,2048]{2,1,0:T(2,128)(2,1)S(1)}, u32[]{:S(2)}, u32[]{:S(2)}) async-start(bf16[16,2,2048]{2,1,0:T(2,128)(2,1)} %broadcast_in_dim.42), calls=%async_computation.2 | async-start | bytes 262144 | tf_op jit(solution)/shard_map/all_to_all | solution.py:23
  54.4 9.9 %all-to-all-start.3 = ((bf16[16,2,128]{2,1,0:T(2,128)(2,1)}), bf16[16,2,128]{2,1,0:T(2,128)(2,1)S(1)}, u32[]{:S(2)}, u32[]{:S(2)}) async-start(bf16[16,2,128]{2,1,0:T(2,128)(2,1)} %bitcast.6), calls=%async_computation.3 | async-start | bytes 16384 | tf_op jit(solution)/shard_map/all_to_all | solution.py:125
  60.1 63.6 %all-gather.3.cloned.1.call-start = ((), (), s32[]{:S(2)}) async-start(), calls=%async_computation.8 | async-start | bytes 2228224 | tf_op jit(solution)/shard_map/all_gather | solution.py:139
  66.1 60.1 %copy-start.11 = (f32[1,128]{1,0:T(1,128)S(1)}, f32[1,128]{1,0:T(1,128)}, u32[]{:S(2)}) copy-start(f32[1,128]{1,0:T(1,128)} %param.39) | copy-start | bytes 1540
  87.5 104.0 %reduce-scatter.2.cloned.1.call-start = ((), (), s32[]{:S(2)}) async-start(), calls=%async_computation.7 | async-start | bytes 2228224 | tf_op jit(solution)/shard_map/reduce_scatter | solution.py:144
  123.7 2.6 %copy-start.1 = (bf16[512,1,2048]{2,0,1:T(8,128)(2,1)S(1)}, bf16[512,1,2048]{2,0,1:T(8,128)(2,1)}, u32[]{:S(2)}) copy-start(bf16[512,1,2048]{2,0,1:T(8,128)(2,1)} %all-gather.3.cloned.1.call-done) | copy-start | bytes 6291460
  130.0 82.8 %copy-start.6 = (f32[2048]{0:T(1024)S(1)}, f32[2048]{0:T(1024)}, u32[]{:S(2)}) copy-start(f32[2048]{0:T(1024)} %param.41) | copy-start | bytes 24580
Sparse Core Ops, SparseCore 0:
  87.6 36.0 all-gather.2
  130.2 61.2 reduce-scatter.1
where the time goes:
time: 221 us; the launch traced here: 220 us
  waiting for transfers between devices  114 us (52%)
  blocking collectives  39.8 us (18%)
  starting transfers between devices  27.3 us (12%)
  between operations  14.3 us (6%)
  matrix products  11.8 us (5%)
  other arithmetic  9.53 us (4%)
  local copies, waits for them, and re-layouts  3.91 us (2%)
    reduce_scatter x1, waiting for transfers between devices, per_device(): lax.psum_scatter(jnp.dot(act, w_down[0], preferred_element_type=jnp.float...  61.4 us
    all_gather x1, waiting for transfers between devices, per_device(): pooled = lax.all_gather(flat, 'tp', axis=0, tiled=True)  36.1 us
    all_to_all x1, blocking collectives, per_device(): lax.all_to_all(outbound, 'ep', split_axis=0, concat_axis=0, tiled=True)  20.5 us
    all_to_all x1, blocking collectives, per_device(): lax.all_to_all(summed.reshape(experts, slots, width), 'ep', split_axis=0,...  19.3 us
    all_to_all x2, starting transfers between devices, sent_to_all(): return lax.all_to_all(copies, axis, split_axis=0, concat_axis=0, tiled=True)  15.7 us
    all_to_all x2, waiting for transfers between devices, sent_to_all(): return lax.all_to_all(copies, axis, split_axis=0, concat_axis=0, tiled=True)  9.28 us
    all_to_all x1, starting transfers between devices, per_device(): lax.all_to_all(gathered, 'tp', split_axis=0, concat_axis=1, tiled=True)  5.75 us
    all_to_all x1, starting transfers between devices, per_device(): lax.all_to_all(projected, 'tp', split_axis=0, concat_axis=1, tiled=True)  5.73 us
  transfers between devices with their start and end apart: 6, of which 6 were waited for; matrix products, arithmetic and copies ran while one was open for 2% of the time, Pallas kernels for 0%

commit v1 on v0

--- a/solution.py
+++ b/solution.py
@@ -136,7 +136,10 @@
     slots = outbound.shape[1]
     arrived = lax.all_to_all(outbound, "ep", split_axis=0, concat_axis=0, tiled=True)
     flat = arrived.reshape(experts * slots, width)
-    pooled = lax.all_gather(flat, "tp", axis=0, tiled=True)
+    n_dev = lax.axis_size("tp")
+    pieces = jnp.stack([flat for _ in range(n_dev)])
+    pieces = lax.all_to_all(pieces, "tp", split_axis=0, concat_axis=0)
+    pooled = jnp.concatenate(pieces, axis=0)
     piece = pooled
     gate = jnp.dot(piece, w_gate[0], preferred_element_type=jnp.float32) + gate_bias[0]
     linear = jnp.dot(piece, w_lin[0], preferred_element_type=jnp.float32) + lin_bias[0]

time: 221 us -> 233 us (1.054)
  blocking collectives: 39.8 us -> 95.7 us
  waiting for transfers between devices: 114 us -> 71.4 us
    all_to_all x0 -> x1, blocking collectives: none -> 56.2 us  [per_device(): pieces = lax.all_to_all(pieces, 'tp', split_axis=0, concat_axis=0)]
    all_gather x1 -> x0, waiting for transfers between devices: 36.1 us -> none  [per_device(): pooled = lax.all_gather(flat, 'tp', axis=0, tiled=True)]
    reduce_scatter x1, waiting for transfers between devices: 61.4 us -> 55.2 us  [per_device(): lax.psum_scatter(jnp.dot(act, w_down[0], preferred_element_type=jnp.float...]
  transfers between devices with their start and end apart: 6 -> 5, of which waited for: 6 -> 5; matrix products, arithmetic and copies ran while one was open for 2% -> 2% of each run, Pallas kernels for 0% -> 0%
where the time goes in v1:
time: 233 us; the launch traced here: 232 us
  blocking collectives  95.7 us (41%)
  waiting for transfers between devices  71.4 us (31%)
  starting transfers between devices  27.3 us (12%)
  between operations  14.3 us (6%)
  matrix products  9.93 us (4%)
  other arithmetic  9.53 us (4%)
  local copies, waits for them, and re-layouts  3.5 us (2%)
    all_to_all x1, blocking collectives, per_device(): pieces = lax.all_to_all(pieces, 'tp', split_axis=0, concat_axis=0)  56.2 us
    reduce_scatter x1, waiting for transfers between devices, per_device(): lax.psum_scatter(jnp.dot(act, w_down[0], preferred_element_type=jnp.float...  55.2 us
    all_to_all x1, blocking collectives, per_device(): lax.all_to_all(outbound, 'ep', split_axis=0, concat_axis=0, tiled=True)  20.5 us
    all_to_all x1, blocking collectives, per_device(): lax.all_to_all(summed.reshape(experts, slots, width), 'ep', split_axis=0,...  19.1 us
    all_to_all x2, starting transfers between devices, sent_to_all(): return lax.all_to_all(copies, axis, split_axis=0, concat_axis=0, tiled=True)  15.7 us
    all_to_all x2, waiting for transfers between devices, sent_to_all(): return lax.all_to_all(copies, axis, split_axis=0, concat_axis=0, tiled=True)  9.28 us
    all_to_all x1, starting transfers between devices, per_device(): lax.all_to_all(gathered, 'tp', split_axis=0, concat_axis=1, tiled=True)  5.75 us
    all_to_all x1, starting transfers between devices, per_device(): lax.all_to_all(projected, 'tp', split_axis=0, concat_axis=1, tiled=True)  5.73 us
  transfers between devices with their start and end apart: 5, of which 5 were waited for; matrix products, arithmetic and copies ran while one was open for 2% of the time, Pallas kernels for 0%

profile of v1, /device:TPU:25, one launch (start us, length us, event | category | flops | bytes accessed | tf_op | source)
XLA Modules:
  0.0 231.7 jit_solution(4501024981146327675)
XLA Ops:
  7.2 1.0 fusion.45
  8.2 0.8 fusion.47
  9.7 9.2 %all-to-all-start = ((bf16[16,2,2048]{2,1,0:T(2,128)(2,1)}), bf16[16,2,2048]{2,1,0:T(2,128)(2,1)S(1)}, u32[]{:S(2)}, u32[]{:S(2)}) async-start(bf16[16,2,2048]{2,1,0:T(2,128)(2,1)} %broadcast_in_dim.37), calls=%async_computation | async-start | bytes 262144 | tf_op jit(solution)/shard_map/all_to_all | solution.py:23
  19.6 0.8 select_reduce_fusion
  20.4 0.8 fusion.55
  21.3 0.8 broadcast_subtract_fusion
  22.1 3.2 %all-to-all-done = bf16[16,2,2048]{2,1,0:T(2,128)(2,1)S(1)} async-done(((bf16[16,2,2048]{2,1,0:T(2,128)(2,1)}), bf16[16,2,2048]{2,1,0:T(2,128)(2,1)S(1)}, u32[]{:S(2)}, u32[]{:S(2)}) %all-to-all-start) | async-done | bytes 131104 | tf_op jit(solution)/shard_map/all_to_all | solution.py:23
  25.2 1.1 convolution_convert_fusion.3
  26.3 1.3 convolution_convert_fusion.4
  28.2 5.8 %all-to-all-start.1 = ((bf16[16,2,160]{2,1,0:T(2,128)(2,1)}), bf16[16,2,160]{2,1,0:T(2,128)(2,1)S(1)}, u32[]{:S(2)}, u32[]{:S(2)}) async-start(bf16[16,2,160]{2,1,0:T(2,128)(2,1)} %copy.44), calls=%async_computation.1 | async-start | bytes 32768 | tf_op jit(solution)/shard_map/all_to_all | solution.py:89
  34.0 0.7 iota_compare_fusion.1
  34.7 0.8 reduce_max.19
  35.5 3.0 %all-to-all-done.1 = bf16[16,2,160]{2,1,0:T(2,128)(2,1)S(1)} async-done(((bf16[16,2,160]{2,1,0:T(2,128)(2,1)}), bf16[16,2,160]{2,1,0:T(2,128)(2,1)S(1)}, u32[]{:S(2)}, u32[]{:S(2)}) %all-to-all-start.1) | async-done | bytes 10272 | tf_op jit(solution)/shard_map/all_to_all | solution.py:89
  40.6 6.6 %all-to-all-start.2 = ((bf16[16,2,2048]{2,1,0:T(2,128)(2,1)}), bf16[16,2,2048]{2,1,0:T(2,128)(2,1)S(1)}, u32[]{:S(2)}, u32[]{:S(2)}) async-start(bf16[16,2,2048]{2,1,0:T(2,128)(2,1)} %broadcast_in_dim.42), calls=%async_computation.2 | async-start | bytes 262144 | tf_op jit(solution)/shard_map/all_to_all | solution.py:23
  47.4 6.1 %all-to-all-done.2 = bf16[16,2,2048]{2,1,0:T(2,128)(2,1)S(1)} async-done(((bf16[16,2,2048]{2,1,0:T(2,128)(2,1)}), bf16[16,2,2048]{2,1,0:T(2,128)(2,1)S(1)}, u32[]{:S(2)}, u32[]{:S(2)}) %all-to-all-start.2) | async-done | bytes 131104 | tf_op jit(solution)/shard_map/all_to_all | solution.py:23
  53.5 0.8 convolution_convert_fusion.2
  54.3 5.7 %all-to-all-start.3 = ((bf16[16,2,128]{2,1,0:T(2,128)(2,1)}), bf16[16,2,128]{2,1,0:T(2,128)(2,1)S(1)}, u32[]{:S(2)}, u32[]{:S(2)}) async-start(bf16[16,2,128]{2,1,0:T(2,128)(2,1)} %bitcast.6), calls=%async_computation.3 | async-start | bytes 16384 | tf_op jit(solution)/shard_map/all_to_all | solution.py:125
  60.2 4.0 %all-to-all-done.3 = bf16[16,2,128]{2,1,0:T(2,128)(2,1)S(1)} async-done(((bf16[16,2,128]{2,1,0:T(2,128)(2,1)}), bf16[16,2,128]{2,1,0:T(2,128)(2,1)S(1)}, u32[]{:S(2)}, u32[]{:S(2)}) %all-to-all-start.3) | async-done | bytes 8224 | tf_op jit(solution)/shard_map/all_to_all | solution.py:125
  66.1 20.5 %all_to_all.51 = bf16[32,2,1024]{2,1,0:T(2,128)(2,1)S(1)} all-to-all(bf16[32,2,1024]{2,1,0:T(2,128)(2,1)S(1)} %reshape.161), channel_id=1, replica_groups=mesh['ep'=32,'tp'=16] {'ep'}, dimensions={0} | all-to-all | bytes 262144 | tf_op jit(solution)/shard_map/all_to_all | solution.py:137
  87.0 56.2 %all_to_all.52 = bf16[16,32,2048]{2,1,0:T(8,128)(2,1)S(1)} all-to-all(bf16[16,32,2048]{2,1,0:T(8,128)(2,1)S(1)} %stack.3), channel_id=1, replica_groups=mesh['ep'=32,'tp'=16] {'tp'}, dimensions={0} | all-to-all | bytes 4194304 | tf_op jit(solution)/shard_map/all_to_all | solution.py:141
  144.0 3.8 %convolution_convert_fusion = bf16[512,2048]{1,0:T(8,128)(2,1)} fusion(bf16[512,2048]{1,0:T(8,128)(2,1)S(1)} %bitcast.84, bf16[1,128,2048]{2,1,0:T(8,128)(2,1)} %param.40, bf16[1,2048,128]{2,1,0:T(8,128)(2,1)} %param.37, f32[512,128]{1,0:T(8,128)S(1)} %fusion.1, f32[128]{0:T(128)S(1)} %bitcast.93), kind=kOutput, calls=%fused_computation | convolution fusion | flops 538574848 | bytes 5505536 | tf_op jit(solution)/shard_map/dot_general | solution.py:148
  147.8 55.2 %reduce-scatter.2.cloned.1.call-done = bf16[32,2048]{1,0:T(8,128)(2,1)} async-done(((bf16[512,2048]{1,0:T(8,128)(2,1)}), bf16[32,2048]{1,0:T(8,128)(2,1)}) %reduce-scatter.2.cloned.1.call-update) | async-done | bytes 131088 | tf_op jit(solution)/shard_map/reduce_scatter | solution.py:147
  203.0 1.6 reduce.3
  204.6 19.1 %all_to_all.53 = bf16[32,2,1024]{2,1,0:T(2,128)(2,1)S(1)} all-to-all(bf16[32,2,1024]{2,1,0:T(2,128)(2,1)S(1)} %reshape.163), channel_id=1, replica_groups=mesh['ep'=32,'tp'=16] {'ep'}, dimensions={0} | all-to-all | bytes 262144 | tf_op jit(solution)/shard_map/all_to_all | solution.py:153
  (70 shorter events, 8.7 us)
Async XLA Ops:
  7.2 31.6 %copy-start = (bf16[2,1024,256]{2,1,0:T(8,128)(2,1)S(1)}, bf16[2,1024,256]{2,1,0:T(8,128)(2,1)}, u32[]{:S(2)}) copy-start(bf16[2,1024,256]{2,1,0:T(8,128)(2,1)} %param.22) | copy-start | bytes 3145732
  7.2 32.3 %copy-start.12 = (bf16[2,1024,256]{2,1,0:T(8,128)(2,1)S(1)}, bf16[2,1024,256]{2,1,0:T(8,128)(2,1)}, u32[]{:S(2)}) copy-start(bf16[2,1024,256]{2,1,0:T(8,128)(2,1)} %param.23) | copy-start | bytes 3145732
  9.7 15.6 %all-to-all-start = ((bf16[16,2,2048]{2,1,0:T(2,128)(2,1)}), bf16[16,2,2048]{2,1,0:T(2,128)(2,1)S(1)}, u32[]{:S(2)}, u32[]{:S(2)}) async-start(bf16[16,2,2048]{2,1,0:T(2,128)(2,1)} %broadcast_in_dim.37), calls=%async_computation | async-start | bytes 262144 | tf_op jit(solution)/shard_map/all_to_all | solution.py:23
  26.3 20.8 %copy-start.4 = (f32[2,4]{1,0:T(2,128)S(1)}, f32[2,4]{1,0:T(2,128)}, u32[]{:S(2)}) copy-start(f32[2,4]{1,0:T(2,128)} %param.27) | copy-start | bytes 100
  27.6 25.9 %copy-start.1 = (bf16[2048,128]{1,0:T(8,128)(2,1)S(1)}, bf16[2048,128]{1,0:T(8,128)(2,1)}, u32[]{:S(2)}) copy-start(bf16[2048,128]{1,0:T(8,128)(2,1)} %param.33) | copy-start | bytes 1572868
  28.2 10.3 %all-to-all-start.1 = ((bf16[16,2,160]{2,1,0:T(2,128)(2,1)}), bf16[16,2,160]{2,1,0:T(2,128)(2,1)S(1)}, u32[]{:S(2)}, u32[]{:S(2)}) async-start(bf16[16,2,160]{2,1,0:T(2,128)(2,1)} %copy.44), calls=%async_computation.1 | async-start | bytes 32768 | tf_op jit(solution)/shard_map/all_to_all | solution.py:89
  38.6 15.7 %copy-start.7 = (bf16[2,512]{1,0:T(2,128)(2,1)}, bf16[2,512]{1,0:T(2,128)(2,1)S(1)}, u32[]{:S(2)}) copy-start(bf16[2,512]{1,0:T(2,128)(2,1)S(1)} %reshape.147) | copy-start | bytes 6148
  38.8 21.3 %copy-start.9 = (s32[2,4]{1,0:T(2,128)S(1)}, s32[2,4]{1,0:T(2,128)}, u32[]{:S(2)}) copy-start(s32[2,4]{1,0:T(2,128)} %param.26) | copy-start | bytes 100
  38.8 25.6 %copy-start.3 = (bf16[2,2048]{1,0:T(2,128)(2,1)S(1)}, bf16[2,2048]{1,0:T(2,128)(2,1)}, u32[]{:S(2)}) copy-start(bf16[2,2048]{1,0:T(2,128)(2,1)} %param.21) | copy-start | bytes 24580
  38.8 25.6 %copy-start.8 = (f32[2048]{0:T(1024)S(1)}, f32[2048]{0:T(1024)}, u32[]{:S(2)}) copy-start(f32[2048]{0:T(1024)} %param.34) | copy-start | bytes 24580
  38.8 25.8 %copy-start.5 = (f32[2048]{0:T(1024)S(1)}, f32[2048]{0:T(1024)}, u32[]{:S(2)}) copy-start(f32[2048]{0:T(1024)} %param.35) | copy-start | bytes 24580
  40.6 12.9 %all-to-all-start.2 = ((bf16[16,2,2048]{2,1,0:T(2,128)(2,1)}), bf16[16,2,2048]{2,1,0:T(2,128)(2,1)S(1)}, u32[]{:S(2)}, u32[]{:S(2)}) async-start(bf16[16,2,2048]{2,1,0:T(2,128)(2,1)} %broadcast_in_dim.42), calls=%async_computation.2 | async-start | bytes 262144 | tf_op jit(solution)/shard_map/all_to_all | solution.py:23
  54.3 9.9 %all-to-all-start.3 = ((bf16[16,2,128]{2,1,0:T(2,128)(2,1)}), bf16[16,2,128]{2,1,0:T(2,128)(2,1)S(1)}, u32[]{:S(2)}, u32[]{:S(2)}) async-start(bf16[16,2,128]{2,1,0:T(2,128)(2,1)} %bitcast.6), calls=%async_computation.3 | async-start | bytes 16384 | tf_op jit(solution)/shard_map/all_to_all | solution.py:125
  60.1 142.9 %reduce-scatter.2.cloned.1.call-start = ((), (), s32[]{:S(2)}) async-start(), calls=%async_computation.8 | async-start | bytes 2228224 | tf_op jit(solution)/shard_map/reduce_scatter | solution.py:147
  87.0 56.2 %copy-start.2 = (bf16[1,2048,128]{2,1,0:T(8,128)(2,1)S(1)}, bf16[1,2048,128]{2,1,0:T(8,128)(2,1)}, u32[]{:S(2)}) copy-start(bf16[1,2048,128]{2,1,0:T(8,128)(2,1)} %param.36) | copy-start | bytes 1572868
  87.0 56.2 %copy-start.10 = (f32[1,128]{1,0:T(1,128)S(1)}, f32[1,128]{1,0:T(1,128)}, u32[]{:S(2)}) copy-start(f32[1,128]{1,0:T(1,128)} %param.38) | copy-start | bytes 1540
  143.2 0.7 copy-start.11
  147.8 76.4 %copy-start.6 = (f32[2048]{0:T(1024)S(1)}, f32[2048]{0:T(1024)}, u32[]{:S(2)}) copy-start(f32[2048]{0:T(1024)} %param.41) | copy-start | bytes 24580
Sparse Core Ops, SparseCore 0:
  147.9 54.9 reduce-scatter.1
